TPU v7x, 128 devices: a whole 4x4x4 slice. The times are simulated.
128 devices in a mesh: gr: 2 (over z_hi), fs: 32 (over z_lo, y, x), tp: 2 (over core).
Axes of the slice: x: 4, y: 4, z: 4 (z_hi: 2, z_lo: 2; z = z_hi * 2 + z_lo), core: 2. Of those that a mesh axis runs over, the one named last changes fastest.
Arguments:
- tokens: bfloat16 [4, 2048, 2048], P(('gr', 'tp')), may hold values from -6 to 6
- gate_master: float32 [3, 2048, 7168], P(None, 'fs', ('gr', 'tp')), may hold values from -0.125 to 0.125
- up_master: float32 [3, 2048, 7168], P(None, 'fs', ('gr', 'tp')), may hold values from -0.125 to 0.125
- down_master: float32 [3, 7168, 2048], P(None, 'fs', ('gr', 'tp')), may hold values from -0.0625 to 0.0625
- norm_gain: float32 [2048], P('fs'), may hold values from 0.1 to 1.9
- route: int32 [4, 2048, 2], P(('gr', 'tp')), may hold values from 0 to 2, all different within a row
- route_weight: float32 [4, 2048, 2], P(('gr', 'tp')), may hold values from 0.05 to 1
Outputs:
- gate_out: bfloat16 [3, 2048, 7168], P(None, None, 'fs')
- up_out: bfloat16 [3, 2048, 7168], P(None, None, 'fs')
- down_out: bfloat16 [3, 7168, 2048], P(None, 'fs')
- mixed: bfloat16 [4, 2048, 2048], P(('gr', 'tp'), 'fs')
Inputs may be any that keep to these rules, and one draw needn't show every extreme that they name: `route`: each token names two different experts; every expert is named by some token.
All inputs are finite; a program needn't handle non-finite values.
Results may differ from a plain program's by a relative error of at most 0.024.
Values may be sent and summed in bfloat16 or wider, within the bound.
No kernel may reach another device: no remote copies, remote signals or barrier semaphores. Data moves between devices by JAX's collectives and lax.ppermute only.
A program may use at most 192 MiB of HBM per device.

v0:
```python
import jax
import jax.numpy as jnp
from jax import lax
from jax.sharding import Mesh
from jax.sharding import PartitionSpec as P

FS = ("fs_0", "fs_1", "fs_2")


def reduced_to_own(blocks, axes, order):
    dims = [lax.axis_size(a) for a in axes]
    blocks = blocks.reshape(*dims, *blocks.shape[1:])
    blocks = blocks.transpose(*order, *range(len(axes), blocks.ndim))
    blocks = blocks.reshape(-1, *blocks.shape[len(axes) :])
    for k in order:
        blocks = lax.psum_scatter(blocks, axes[k], scatter_dimension=0, tiled=True)
    return blocks[0]


def split_up(array, dim, peers):
    dims = array.shape
    blocks = array.reshape(*dims[:dim], peers, dims[dim] // peers, *dims[dim + 1 :])
    return jnp.moveaxis(blocks, dim, 0)


def sum_by_axis_2(array, axes, order, dim):
    peers = lax.axis_size(axes)
    return reduced_to_own(split_up(array, dim, peers), axes, order)


def normalize(rows_in):
    values = rows_in.astype(jnp.float32)
    scaled = values * lax.rsqrt(jnp.mean(values * values, axis=-1, keepdims=True) + 1e-06)
    return scaled.astype(jnp.bfloat16)


def mixing(chosen, weights, experts):
    share = weights / jnp.sum(weights, axis=-1, keepdims=True)
    labels = jnp.arange(experts, dtype=jnp.int32)
    match = (chosen[:, :, None] == labels[None, None, :]).astype(jnp.float32)
    return jnp.sum(share[:, :, None] * match, axis=1)


def expert_term(normed, mix_column, gate_weight, up_weight, down_weight):
    gate_act = jnp.dot(normed, gate_weight, preferred_element_type=jnp.float32)
    up_act = jnp.dot(normed, up_weight, preferred_element_type=jnp.float32)
    hidden = (jax.nn.silu(gate_act) * up_act).astype(jnp.bfloat16)
    projected = jnp.dot(hidden, down_weight, preferred_element_type=jnp.float32)
    return mix_column * projected


def shards(tokens, gate_master, up_master, down_master, norm_gain, route, route_weight):
    scaled_gain = norm_gain[None, :, None]
    gate_local = (scaled_gain * gate_master).astype(jnp.bfloat16)
    up_local = (scaled_gain * up_master).astype(jnp.bfloat16)
    down_local = down_master.astype(jnp.bfloat16)
    experts = gate_local.shape[0]
    normed = normalize(tokens[0])
    combine = mixing(route[0], route_weight[0], experts)
    width = normed.shape[1]
    gate_rows, up_rows, down_out = (
        lax.all_gather(gate_local, ("gr", "tp"), axis=2, tiled=True),
        lax.all_gather(up_local, ("gr", "tp"), axis=2, tiled=True),
        lax.all_gather(down_local, ("gr", "tp"), axis=2, tiled=True),
    )
    gate_out, up_out = (
        lax.all_to_all(gate_rows, FS, split_axis=2, concat_axis=1, tiled=True),
        lax.all_to_all(up_rows, FS, split_axis=2, concat_axis=1, tiled=True),
    )
    own_rows = normed.shape[0] // lax.axis_size(FS)
    total = jnp.zeros((own_rows * lax.axis_size(FS), width), jnp.float32)
    for index in range(experts):
        total = total + expert_term(
            normed, combine[:, index : index + 1], gate_out[index], up_out[index], down_out[index]
        )
    summed = sum_by_axis_2(total.astype(jnp.bfloat16), FS, (1, 2, 0), 0).astype(jnp.float32)
    mixed = summed.astype(jnp.bfloat16)[None]
    return (gate_out, up_out, down_out, mixed)


def solution(mesh):
    split = Mesh(
        mesh.devices.reshape(mesh.shape["gr"], 2, 4, 4, mesh.shape["tp"]),
        ("gr", "fs_0", "fs_1", "fs_2", "tp"),
    )
    in_specs = (
        P(("gr", "tp"), None, None),
        P(None, FS, ("gr", "tp")),
        P(None, FS, ("gr", "tp")),
        P(None, FS, ("gr", "tp")),
        P(FS),
        P(("gr", "tp"), None, None),
        P(("gr", "tp"), None, None),
    )
    out_specs = (P(None, None, FS), P(None, None, FS), P(None, FS, None), P(("gr", "tp"), FS, None))
    return jax.shard_map(
        shards, mesh=split, in_specs=in_specs, out_specs=out_specs, check_vma=False
    )
```

profile of v0, /device:TPU:1, one launch (start us, length us, event | category | flops | bytes accessed | tf_op | source)
XLA Modules:
  0.0 390.9 jit_solution(5299467397481243480)
XLA Ops:
  7.2 0.0 all-gather.4.cloned.1.call-start
  7.2 3.1 multiply_convert_fusion
  10.3 0.0 all-gather.4.cloned.1.call-update
  10.3 0.0 all-gather.6.cloned.1.call-start
  10.4 0.7 all-gather.6.cloned.1.call-update
  11.1 33.5 %all-gather.4.cloned.1.call-done = bf16[3,64,7168]{2,1,0:T(8,128)(2,1)} async-done(((bf16[3,64,1792]{2,1,0:T(8,128)(2,1)}), bf16[3,64,7168]{2,1,0:T(8,128)(2,1)}) %all-gather.4.cloned.1.call-update) | async-done | bytes 2752528 | tf_op jit(solution)/shard_map/all_gather | solution.py:62
  44.5 10.1 %copy.41 = bf16[3,64,7168]{1,0,2:T(4,128)(2,1)} copy(bf16[3,64,7168]{2,1,0:T(8,128)(2,1)} %all-gather.4.cloned.1.call-done) | data formatting | bytes 5505024 | tf_op jit(solution)/shard_map/all_gather | solution.py:62
  54.6 12.6 %reshape.105 = bf16[32,2,21504]{2,1,0:T(2,128)(2,1)} reshape(bf16[7168,3,64]{2,1,0:T(4,128)(2,1)} %bitcast.55) | data formatting | bytes 5505024
  67.2 7.0 %all-to-all-start = ((bf16[32,2,21504]{2,1,0:T(2,128)(2,1)}), bf16[32,2,21504]{2,1,0:T(2,128)(2,1)S(1)}, u32[]{:S(2)}, u32[]{:S(2)}) async-start(bf16[32,2,21504]{2,1,0:T(2,128)(2,1)} %reshape.105), calls=%async_computation | async-start | bytes 5505024 | tf_op jit(solution)/shard_map/all_to_all | solution.py:67
  74.3 0.0 copy-start.2
  74.3 0.0 all-gather.8.cloned.1.call-start
  74.3 2.3 convert_element_type.47
  76.6 0.0 all-gather.8.cloned.1.call-update
  76.6 0.0 copy-done.2
  76.7 0.0 all-gather.6.cloned.1.call-done
  76.7 10.1 %copy.43 = bf16[3,64,7168]{1,0,2:T(4,128)(2,1)} copy(bf16[3,64,7168]{2,1,0:T(8,128)(2,1)} %all-gather.6.cloned.1.call-done) | data formatting | bytes 5505024 | tf_op jit(solution)/shard_map/all_gather | solution.py:63
  86.8 12.6 %reshape.107 = bf16[32,2,21504]{2,1,0:T(2,128)(2,1)} reshape(bf16[7168,3,64]{2,1,0:T(4,128)(2,1)} %bitcast.56) | data formatting | bytes 5505024
  99.4 0.0 copy-start.3
  99.4 9.2 %all-to-all-done = bf16[32,2,21504]{2,1,0:T(2,128)(2,1)S(1)} async-done(((bf16[32,2,21504]{2,1,0:T(2,128)(2,1)}), bf16[32,2,21504]{2,1,0:T(2,128)(2,1)S(1)}, u32[]{:S(2)}, u32[]{:S(2)}) %all-to-all-start) | async-done | bytes 2752544 | tf_op jit(solution)/shard_map/all_to_all | solution.py:67
  108.6 6.3 %all-to-all-start.1 = ((bf16[32,2,21504]{2,1,0:T(2,128)(2,1)}), bf16[32,2,21504]{2,1,0:T(2,128)(2,1)}, u32[]{:S(2)}, u32[]{:S(2)}) async-start(bf16[32,2,21504]{2,1,0:T(2,128)(2,1)} %reshape.107), calls=%async_computation.1 | async-start | bytes 5505024 | tf_op jit(solution)/shard_map/all_to_all | solution.py:68
  115.0 0.0 reduce-scatter.4.cloned.1.call-start
  115.0 0.0 copy-done.3
  115.0 0.1 fusion.20
  115.1 5.1 %fusion = f32[2048]{0:T(1024)S(1)} fusion(bf16[1,2048,2048]{2,1,0:T(8,128)(2,1)} %param.7), kind=kLoop, calls=%fused_computation.2 | loop fusion | flops 12580864 | bytes 8396800 | tf_op jit(solution)/shard_map/reduce_sum | solution.py:33
  120.3 8.0 %fusion.2 = bf16[2048,2048]{1,0:T(8,128)(2,1)} fusion(bf16[1,2048,2048]{2,1,0:T(8,128)(2,1)} %param.7, f32[2048]{0:T(1024)S(1)} %add_rsqrt_fusion), kind=kLoop, calls=%fused_computation.5 | loop fusion | flops 12582912 | bytes 16785408 | tf_op jit(solution)/shard_map/convert_element_type | solution.py:34
  128.3 8.7 %reshape.106 = bf16[7168,3,64]{2,1,0:T(4,128)(2,1)} reshape(bf16[32,2,21504]{2,1,0:T(2,128)(2,1)S(1)} %all-to-all-done) | data formatting | bytes 5505024
  136.9 10.7 %copy.42 = bf16[3,64,32,224]{3,1,2,0:T(8,128)(2,1)S(1)} copy(bf16[3,64,32,224]{1,0,3,2:T(4,128)(2,1)} %bitcast.57) | data formatting | bytes 5505024 | tf_op jit(solution)/shard_map/all_to_all | solution.py:67
  147.7 0.9 all-to-all-done.1
  148.6 12.5 %reshape.108 = bf16[7168,3,64]{2,1,0:T(4,128)(2,1)} reshape(bf16[32,2,21504]{2,1,0:T(2,128)(2,1)} %all-to-all-done.1) | data formatting | bytes 5505024
  161.0 11.4 %copy.44 = bf16[3,64,32,224]{3,1,2,0:T(8,128)(2,1)} copy(bf16[3,64,32,224]{1,0,3,2:T(4,128)(2,1)} %bitcast.58) | data formatting | bytes 5505024 | tf_op jit(solution)/shard_map/all_to_all | solution.py:68
  172.4 0.0 copy-start
  172.4 0.2 fusion.24
  172.6 1.7 copy-done
  174.3 0.0 slice-start
  174.3 1.8 fusion.25
  176.1 0.0 slice-start.1
  176.1 8.0 %fusion.27 = f32[2048,224]{0,1:T(8,128)} fusion(bf16[2048,2048]{1,0:T(8,128)(2,1)} %fusion.2, bf16[2048,224]{1,0:T(8,128)(2,1)S(1)} %bitcast.68), kind=kOutput, calls=%fused_computation.41 | convolution fusion | flops 1879048192 | bytes 11141120 | tf_op jit(solution)/shard_map/dot_general | solution.py:45
  184.1 0.0 slice-done
  184.1 0.0 slice-done.1
  184.1 4.0 %fusion.28 = f32[2048,224]{0,1:T(8,128)} fusion(bf16[2048,2048]{1,0:T(8,128)(2,1)S(1)} %bitcast.52, bf16[2048,224]{1,0:T(8,128)(2,1)S(1)} %bitcast.67), kind=kOutput, calls=%fused_computation.42 | convolution fusion | flops 1879048192 | bytes 11141120 | tf_op jit(solution)/shard_map/dot_general | solution.py:45
  188.1 4.0 %fusion.29 = f32[2048,224]{0,1:T(8,128)} fusion(bf16[2048,2048]{1,0:T(8,128)(2,1)S(1)} %bitcast.52, bf16[2048,224]{1,0:T(8,128)(2,1)S(1)} %bitcast.66), kind=kOutput, calls=%fused_computation.43 | convolution fusion | flops 1879048192 | bytes 11141120 | tf_op jit(solution)/shard_map/dot_general | solution.py:45
  192.1 0.0 all-gather.8.cloned.1.call-done
  192.1 15.3 %fusion.7 = f32[2048,2048]{1,0:T(8,128)} fusion(bf16[2048,2048]{1,0:T(8,128)(2,1)} %fusion.2, bf16[2048,224]{1,0:T(8,128)(2,1)} %bitcast.64, f32[2048,224]{0,1:T(8,128)} %fusion.27, bf16[3,224,2048]{2,1,0:T(8,128)(2,1)} %all-gather.8.cloned.1.call-done), kind=kOutput, calls=%fused_computation.13 | convolution fusion | flops 3760848896 | bytes 28966912 | tf_op jit(solution)/shard_map/dot_general | solution.py:48
  207.4 15.5 %fusion.6 = f32[2048,2048]{1,0:T(8,128)} fusion(bf16[2048,2048]{1,0:T(8,128)(2,1)} %fusion.2, bf16[2048,224]{1,0:T(8,128)(2,1)} %bitcast.63, f32[2048,224]{0,1:T(8,128)} %fusion.28, bf16[3,224,2048]{2,1,0:T(8,128)(2,1)} %all-gather.8.cloned.1.call-done), kind=kOutput, calls=%fused_computation.12 | convolution fusion | flops 3760848896 | bytes 28966912 | tf_op jit(solution)/shard_map/dot_general | solution.py:48
  222.9 19.2 %add_convert_fusion = bf16[2048,2048]{1,0:T(8,128)(2,1)} fusion(f32[2048,2048]{1,0:T(8,128)} %fusion.6, f32[2048,2048]{1,0:T(8,128)} %fusion.7, f32[2048]{0:T(1024)S(1)} %bitcast.70, f32[2048]{0:T(1024)S(1)} %bitcast.71, f32[2048]{0:T(1024)S(1)} %bitcast.69, bf16[3,224,2048]{2,1,0:T(8,128)(2,1)} %all-gather.8.cloned.1.call-done, ...), kind=kOutput, calls=%fused_computation.4 | convolution fusion | flops 3786014720 | bytes 54157312 | tf_op jit(solution)/shard_map/dot_general | solution.py:48
  242.0 8.3 %copy.45 = bf16[4,4,2,64,2048]{4,3,2,1,0:T(8,128)(2,1)} copy(bf16[4,4,2,64,2048]{4,3,1,0,2:T(8,128)(2,1)} %bitcast.54) | data formatting | bytes 16777216 | tf_op jit(solution)/shard_map/transpose | solution.py:13
  250.3 0.0 reduce-scatter.4.cloned.1.call-update
  250.3 0.0 reduce-scatter.6.cloned.1.call-start
  250.4 80.8 %reduce-scatter.4.cloned.1.call-done = bf16[8,64,2048]{2,1,0:T(8,128)(2,1)} async-done(((bf16[32,64,2048]{2,1,0:T(8,128)(2,1)}), bf16[8,64,2048]{2,1,0:T(8,128)(2,1)}) %reduce-scatter.4.cloned.1.call-update) | async-done | bytes 2097168 | tf_op jit(solution)/shard_map/reduce_scatter | solution.py:16
  331.2 0.0 reduce-scatter.6.cloned.1.call-update
  331.2 0.0 reduce-scatter.8.cloned.1.call-start
  331.3 31.6 %reduce-scatter.6.cloned.1.call-done = bf16[2,64,2048]{2,1,0:T(8,128)(2,1)} async-done(((bf16[8,64,2048]{2,1,0:T(8,128)(2,1)}), bf16[2,64,2048]{2,1,0:T(8,128)(2,1)}) %reduce-scatter.6.cloned.1.call-update) | async-done | bytes 524304 | tf_op jit(solution)/shard_map/reduce_scatter | solution.py:16
  362.9 0.0 reduce-scatter.8.cloned.1.call-update
  362.9 2.7 copy.46
  365.6 0.0 copy-start.1
  365.6 4.7 %copy.47 = bf16[3,2048,224]{1,2,0:T(8,128)(2,1)} copy(bf16[3,2048,224]{2,1,0:T(8,128)(2,1)} %bitcast.61) | data formatting | bytes 5505024
  370.3 12.2 %reduce-scatter.8.cloned.1.call-done = bf16[1,64,2048]{2,1,0:T(8,128)(2,1)} async-done(((bf16[2,64,2048]{2,1,0:T(8,128)(2,1)}), bf16[1,64,2048]{2,1,0:T(8,128)(2,1)}) %reduce-scatter.8.cloned.1.call-update) | async-done | bytes 262160 | tf_op jit(solution)/shard_map/reduce_scatter | solution.py:16
  382.5 0.0 copy-done.1
  382.5 1.5 copy.49
  (5 shorter events, 0.1 us)
Async XLA Ops:
  7.2 37.4 %all-gather.4.cloned.1.call-start = ((), (), s32[]{:S(2)}) async-start(), calls=%async_computation.5 | async-start | bytes 3440640 | tf_op jit(solution)/shard_map/all_gather | solution.py:62
  10.3 66.4 %all-gather.6.cloned.1.call-start = ((), (), s32[]{:S(2)}) async-start(), calls=%async_computation.6 | async-start | bytes 3440640 | tf_op jit(solution)/shard_map/all_gather | solution.py:63
  67.2 41.4 %all-to-all-start = ((bf16[32,2,21504]{2,1,0:T(2,128)(2,1)}), bf16[32,2,21504]{2,1,0:T(2,128)(2,1)S(1)}, u32[]{:S(2)}, u32[]{:S(2)}) async-start(bf16[32,2,21504]{2,1,0:T(2,128)(2,1)} %reshape.105), calls=%async_computation | async-start | bytes 5505024 | tf_op jit(solution)/shard_map/all_to_all | solution.py:67
  74.3 2.4 copy-start.2
  74.3 117.9 %all-gather.8.cloned.1.call-start = ((), (), s32[]{:S(2)}) async-start(), calls=%async_computation.7 | async-start | bytes 3440640 | tf_op jit(solution)/shard_map/all_gather | solution.py:64
  99.4 15.6 %copy-start.3 = (s32[1,2048,2]{1,2,0:T(2,128)S(1)}, s32[1,2048,2]{1,2,0:T(2,128)}, u32[]{:S(2)}) copy-start(s32[1,2048,2]{1,2,0:T(2,128)} %param.12) | copy-start | bytes 49156
  108.6 39.9 %all-to-all-start.1 = ((bf16[32,2,21504]{2,1,0:T(2,128)(2,1)}), bf16[32,2,21504]{2,1,0:T(2,128)(2,1)}, u32[]{:S(2)}, u32[]{:S(2)}) async-start(bf16[32,2,21504]{2,1,0:T(2,128)(2,1)} %reshape.107), calls=%async_computation.1 | async-start | bytes 5505024 | tf_op jit(solution)/shard_map/all_to_all | solution.py:68
  115.0 216.3 %reduce-scatter.4.cloned.1.call-start = ((), (), s32[]{:S(2)}) async-start(), calls=%async_computation.8 | async-start | bytes 10485760 | tf_op jit(solution)/shard_map/reduce_scatter | solution.py:16
  172.4 1.9 copy-start
  174.3 9.8 %slice-start = ((s8[8388608]{0:T(1024)(128)(4,1)}), s8[4194304]{0:T(1024)(128)(4,1)S(1)}, s32[]{:S(2)}) async-start(s8[8388608]{0:T(1024)(128)(4,1)} %bitcast.51), calls=%async_computation.11 | async-start | bytes 8388608
  176.1 8.0 %slice-start.1 = ((s8[8388608]{0:T(1024)(128)(4,1)}), s8[4194304]{0:T(1024)(128)(4,1)S(1)}, s32[]{:S(2)}) async-start(s8[8388608]{0:T(1024)(128)(4,1)} %bitcast.51), calls=%async_computation.12 | async-start | bytes 8388608
  250.3 112.5 %reduce-scatter.6.cloned.1.call-start = ((), (), s32[]{:S(2)}) async-start(), calls=%async_computation.9 | async-start | bytes 2621440 | tf_op jit(solution)/shard_map/reduce_scatter | solution.py:16
  331.2 51.3 %reduce-scatter.8.cloned.1.call-start = ((), (), s32[]{:S(2)}) async-start(), calls=%async_computation.10 | async-start | bytes 786432 | tf_op jit(solution)/shard_map/reduce_scatter | solution.py:16
  365.6 16.9 %copy-start.1 = (bf16[3,224,2048]{2,1,0:T(8,128)(2,1)S(1)}, bf16[3,224,2048]{2,1,0:T(8,128)(2,1)}, u32[]{:S(2)}) copy-start(bf16[3,224,2048]{2,1,0:T(8,128)(2,1)} %all-gather.8.cloned.1.call-done) | copy-start | bytes 8257540
Sparse Core Ops, SparseCore 0:
  10.4 34.0 all-gather.3
  46.8 29.6 all-gather.5
  78.1 74.4 all-gather.7
  250.5 80.7 reduce-scatter.3
  333.5 29.3 reduce-scatter.5
  365.6 16.8 reduce-scatter.7
where the time goes:
time: 393 us; the launch traced here: 391 us
  waiting for transfers between devices  169 us (43%)
  local copies, waits for them, and re-layouts  110 us (28%)
  matrix products  65.9 us (17%)
  other arithmetic  18.6 us (5%)
  between operations  14.2 us (4%)
  starting transfers between devices  13.6 us (3%)
    reduce_scatter x3, waiting for transfers between devices, reduced_to_own(): blocks = lax.psum_scatter(blocks, axes[k], scatter_dimension=0, tiled=True)  125 us
    unnamed x19, local copies, waits for them, and re-layouts  57 us
    dot_general x3, matrix products, expert_term(): projected = jnp.dot(hidden, down_weight, preferred_element_type=jnp.float32)  49.9 us
    all_gather x1, waiting for transfers between devices, shards(): lax.all_gather(gate_local, ('gr', 'tp'), axis=2, tiled=True)  33.5 us
    dot_general x3, matrix products, expert_term(): gate_act = jnp.dot(normed, gate_weight, preferred_element_type=jnp.float32)  16 us
    all_to_all x1, local copies, waits for them, and re-layouts, shards(): lax.all_to_all(up_rows, FS, split_axis=2, concat_axis=1, tiled=True)  11.4 us
    all_to_all x1, local copies, waits for them, and re-layouts, shards(): lax.all_to_all(gate_rows, FS, split_axis=2, concat_axis=1, tiled=True)  10.7 us
    all_gather x1, local copies, waits for them, and re-layouts, shards(): lax.all_gather(up_local, ('gr', 'tp'), axis=2, tiled=True)  10.1 us
  transfers between devices with their start and end apart: 8, of which 6 were waited for; matrix products, arithmetic and copies ran while one was open for 33% of the time, Pallas kernels for 0%

commit v1 on v0

--- a/solution.py
+++ b/solution.py
@@ -59,7 +59,12 @@
     combine = mixing(route[0], route_weight[0], experts)
     width = normed.shape[1]
     gate_rows, up_rows, down_out = (
-        lax.all_gather(gate_local, ("gr", "tp"), axis=2, tiled=True),
+        jnp.concatenate(
+            lax.all_to_all(
+                jnp.stack([gate_local] * lax.axis_size(("gr", "tp"))), ("gr", "tp"), 0, 0
+            ),
+            axis=2,
+        ),
         lax.all_gather(up_local, ("gr", "tp"), axis=2, tiled=True),
         lax.all_gather(down_local, ("gr", "tp"), axis=2, tiled=True),
     )

time: 393 us -> 401 us (1.020)
  local copies, waits for them, and re-layouts: 110 us -> 119 us
  waiting for transfers between devices: 169 us -> 160 us
  starting transfers between devices: 13.6 us -> 22.5 us
    all_to_all x0 -> x1, waiting for transfers between devices: none -> 45.6 us  [shards(): lax.all_to_all(jnp.stack([gate_local] * lax.axis_size(('gr', 'tp'))), ('g...]
    all_gather x1 -> x0, waiting for transfers between devices: 33.5 us -> none  [shards(): lax.all_gather(gate_local, ('gr', 'tp'), axis=2, tiled=True)]
    reduce_scatter x3, waiting for transfers between devices: 125 us -> 114 us  [reduced_to_own(): blocks = lax.psum_scatter(blocks, axes[k], scatter_dimension=0, tiled=True)]
    all_gather x1 -> x0, local copies, waits for them, and re-layouts: 10.1 us -> none  [shards(): lax.all_gather(gate_local, ('gr', 'tp'), axis=2, tiled=True)]
    all_to_all x1, waiting for transfers between devices: 9.23 us -> 0.01 us  [shards(): lax.all_to_all(gate_rows, FS, split_axis=2, concat_axis=1, tiled=True)]
    all_to_all x1 -> x2, local copies, waits for them, and re-layouts: 10.7 us -> 19.4 us  [shards(): lax.all_to_all(gate_rows, FS, split_axis=2, concat_axis=1, tiled=True)]
    reshape x0 -> x1, local copies, waits for them, and re-layouts: none -> 7.43 us  [shards(): jnp.concatenate(lax.all_to_all(jnp.stack([gate_local] * lax.axis_size(('g...]
    all_to_all x0 -> x1, starting transfers between devices: none -> 6.64 us  [shards(): lax.all_to_all(jnp.stack([gate_local] * lax.axis_size(('gr', 'tp'))), ('g...]
  transfers between devices with their start and end apart: 8 -> 8, of which waited for: 6 -> 4; matrix products, arithmetic and copies ran while one was open for 33% -> 35% of each run, Pallas kernels for 0% -> 0%
where the time goes in v1:
time: 401 us; the launch traced here: 399 us
  waiting for transfers between devices  160 us (40%)
  local copies, waits for them, and re-layouts  119 us (30%)
  matrix products  65.4 us (16%)
  starting transfers between devices  22.5 us (6%)
  other arithmetic  18.4 us (5%)
  between operations  13.9 us (3%)
    reduce_scatter x3, waiting for transfers between devices, reduced_to_own(): blocks = lax.psum_scatter(blocks, axes[k], scatter_dimension=0, tiled=True)  114 us
    unnamed x15, local copies, waits for them, and re-layouts  57.2 us
    dot_general x3, matrix products, expert_term(): projected = jnp.dot(hidden, down_weight, preferred_element_type=jnp.float32)  49.6 us
    all_to_all x1, waiting for transfers between devices, shards(): lax.all_to_all(jnp.stack([gate_local] * lax.axis_size(('gr', 'tp'))), ('g...  45.6 us
    all_to_all x2, local copies, waits for them, and re-layouts, shards(): lax.all_to_all(gate_rows, FS, split_axis=2, concat_axis=1, tiled=True)  19.4 us
    dot_general x3, matrix products, expert_term(): gate_act = jnp.dot(normed, gate_weight, preferred_element_type=jnp.float32)  15.7 us
    all_to_all x1, local copies, waits for them, and re-layouts, shards(): lax.all_to_all(up_rows, FS, split_axis=2, concat_axis=1, tiled=True)  10.9 us
    all_gather x1, local copies, waits for them, and re-layouts, shards(): lax.all_gather(up_local, ('gr', 'tp'), axis=2, tiled=True)  10 us
  transfers between devices with their start and end apart: 8, of which 4 were waited for; matrix products, arithmetic and copies ran while one was open for 35% of the time, Pallas kernels for 0%

profile of v1, /device:TPU:1, one launch (start us, length us, event | category | flops | bytes accessed | tf_op | source)
XLA Modules:
  0.0 399.0 jit_solution(12961590832164350112)
XLA Ops:
  7.2 0.0 all-gather.3.cloned.1.call-start
  7.2 2.9 multiply_convert_fusion
  10.1 0.0 all-gather.3.cloned.1.call-update
  10.1 1.8 stack.2
  11.9 6.6 %all-to-all-start = ((bf16[4,3,64,1792]{3,2,1,0:T(8,128)(2,1)}), bf16[4,3,64,1792]{3,2,1,0:T(8,128)(2,1)S(1)}, u32[]{:S(2)}, u32[]{:S(2)}) async-start(bf16[4,3,64,1792]{3,2,1,0:T(8,128)(2,1)} %stack.2), calls=%async_computation | async-start | bytes 5505024 | tf_op jit(solution)/shard_map/all_to_all | solution.py:63
  18.5 0.0 copy-start
  18.5 0.0 all-gather.5.cloned.1.call-start
  18.5 2.3 convert_element_type.47
  20.8 0.0 all-gather.5.cloned.1.call-update
  20.9 0.0 copy-done
  20.9 45.6 %all-to-all-done = bf16[4,3,64,1792]{3,2,1,0:T(8,128)(2,1)S(1)} async-done(((bf16[4,3,64,1792]{3,2,1,0:T(8,128)(2,1)}), bf16[4,3,64,1792]{3,2,1,0:T(8,128)(2,1)S(1)}, u32[]{:S(2)}, u32[]{:S(2)}) %all-to-all-start) | async-done | bytes 2752544 | tf_op jit(solution)/shard_map/all_to_all | solution.py:63
  66.5 7.4 %copy.67 = bf16[3,64,4,1792]{1,0,3,2:T(4,128)(2,1)} copy(bf16[3,64,4,1792]{3,1,0,2:T(8,128)(2,1)S(1)} %bitcast.67) | data formatting | bytes 5505024 | tf_op jit(solution)/shard_map/reshape | solution.py:62
  73.9 12.6 %reshape.115 = bf16[32,2,21504]{2,1,0:T(2,128)(2,1)} reshape(bf16[7168,3,64]{2,1,0:T(4,128)(2,1)} %bitcast.60) | data formatting | bytes 5505024
  86.5 0.0 copy-start.1
  86.5 7.7 %all-to-all-start.1 = ((bf16[32,2,21504]{2,1,0:T(2,128)(2,1)}), bf16[32,2,21504]{2,1,0:T(2,128)(2,1)S(1)}, u32[]{:S(2)}, u32[]{:S(2)}) async-start(bf16[32,2,21504]{2,1,0:T(2,128)(2,1)} %reshape.115), calls=%async_computation.1 | async-start | bytes 5505024 | tf_op jit(solution)/shard_map/all_to_all | solution.py:72
  94.2 0.0 copy-done.1
  94.2 0.1 fusion.20
  94.3 5.1 %fusion = f32[2048]{0:T(1024)S(1)} fusion(bf16[1,2048,2048]{2,1,0:T(8,128)(2,1)} %param.7), kind=kLoop, calls=%fused_computation.2 | loop fusion | flops 12580864 | bytes 8396800 | tf_op jit(solution)/shard_map/reduce_sum | solution.py:33
  99.4 8.0 %fusion.2 = bf16[2048,2048]{1,0:T(8,128)(2,1)} fusion(bf16[1,2048,2048]{2,1,0:T(8,128)(2,1)} %param.7, f32[2048]{0:T(1024)S(1)} %add_rsqrt_fusion), kind=kLoop, calls=%fused_computation.5 | loop fusion | flops 12582912 | bytes 16785408 | tf_op jit(solution)/shard_map/convert_element_type | solution.py:34
  107.4 0.0 all-gather.3.cloned.1.call-done
  107.4 10.0 %copy.59 = bf16[3,64,7168]{1,0,2:T(4,128)(2,1)} copy(bf16[3,64,7168]{2,1,0:T(8,128)(2,1)} %all-gather.3.cloned.1.call-done) | data formatting | bytes 5505024 | tf_op jit(solution)/shard_map/all_gather | solution.py:68
  117.4 12.6 %reshape.117 = bf16[32,2,21504]{2,1,0:T(2,128)(2,1)} reshape(bf16[7168,3,64]{2,1,0:T(4,128)(2,1)} %bitcast.61) | data formatting | bytes 5505024
  130.0 0.0 all-to-all-done.1
  130.0 7.9 %all-to-all-start.2 = ((bf16[32,2,21504]{2,1,0:T(2,128)(2,1)}), bf16[32,2,21504]{2,1,0:T(2,128)(2,1)}, u32[]{:S(2)}, u32[]{:S(2)}) async-start(bf16[32,2,21504]{2,1,0:T(2,128)(2,1)} %reshape.117), calls=%async_computation.2 | async-start | bytes 5505024 | tf_op jit(solution)/shard_map/all_to_all | solution.py:73
  137.9 0.2 reduce-scatter.4.cloned.1.call-start
  138.1 8.7 %reshape.116 = bf16[7168,3,64]{2,1,0:T(4,128)(2,1)} reshape(bf16[32,2,21504]{2,1,0:T(2,128)(2,1)S(1)} %all-to-all-done.1) | data formatting | bytes 5505024
  146.8 8.1 %copy.68 = bf16[3,64,32,224]{3,2,1,0:T(8,128)(2,1)S(1)} copy(bf16[3,64,32,224]{1,0,3,2:T(4,128)(2,1)} %bitcast.56) | data formatting | bytes 5505024 | tf_op jit(solution)/shard_map/all_to_all | solution.py:72
  154.9 0.3 fusion.24
  155.2 0.6 copy.63
  155.8 0.6 copy.62
  156.4 0.0 slice-start
  156.4 0.6 copy.61
  157.0 0.0 slice-start.1
  157.0 7.7 %fusion.29 = f32[2048,224]{0,1:T(8,128)} fusion(bf16[2048,2048]{1,0:T(8,128)(2,1)} %fusion.2, bf16[2048,224]{1,0:T(8,128)(2,1)S(1)} %bitcast.71), kind=kOutput, calls=%fused_computation.43 | convolution fusion | flops 1879048192 | bytes 11141120 | tf_op jit(solution)/shard_map/dot_general | solution.py:45
  164.7 0.0 slice-done
  164.7 0.0 slice-done.1
  164.7 4.0 %fusion.28 = f32[2048,224]{0,1:T(8,128)} fusion(bf16[2048,2048]{1,0:T(8,128)(2,1)S(1)} %bitcast.55, bf16[2048,224]{1,0:T(8,128)(2,1)S(1)} %bitcast.72), kind=kOutput, calls=%fused_computation.42 | convolution fusion | flops 1879048192 | bytes 11141120 | tf_op jit(solution)/shard_map/dot_general | solution.py:45
  168.7 4.0 %fusion.27 = f32[2048,224]{0,1:T(8,128)} fusion(bf16[2048,2048]{1,0:T(8,128)(2,1)S(1)} %bitcast.55, bf16[2048,224]{1,0:T(8,128)(2,1)S(1)} %bitcast.73), kind=kOutput, calls=%fused_computation.41 | convolution fusion | flops 1879048192 | bytes 11141120 | tf_op jit(solution)/shard_map/dot_general | solution.py:45
  172.7 0.0 all-to-all-done.2
  172.7 12.5 %reshape.118 = bf16[7168,3,64]{2,1,0:T(4,128)(2,1)} reshape(bf16[32,2,21504]{2,1,0:T(2,128)(2,1)} %all-to-all-done.2) | data formatting | bytes 5505024
  185.2 10.9 %copy.60 = bf16[3,64,32,224]{3,1,2,0:T(8,128)(2,1)S(1)} copy(bf16[3,64,32,224]{1,0,3,2:T(4,128)(2,1)} %bitcast.62) | data formatting | bytes 5505024 | tf_op jit(solution)/shard_map/all_to_all | solution.py:73
  196.1 1.8 fusion.25
  197.9 0.0 all-gather.5.cloned.1.call-done
  197.9 15.2 %fusion.7 = f32[2048,2048]{1,0:T(8,128)} fusion(bf16[2048,2048]{1,0:T(8,128)(2,1)} %fusion.2, bf16[2048,224]{1,0:T(8,128)(2,1)} %bitcast.69, f32[2048,224]{0,1:T(8,128)} %fusion.27, bf16[3,224,2048]{2,1,0:T(8,128)(2,1)} %all-gather.5.cloned.1.call-done), kind=kOutput, calls=%fused_computation.13 | convolution fusion | flops 3760848896 | bytes 28966912 | tf_op jit(solution)/shard_map/dot_general | solution.py:48
  213.2 15.2 %fusion.6 = f32[2048,2048]{1,0:T(8,128)} fusion(bf16[2048,2048]{1,0:T(8,128)(2,1)} %fusion.2, bf16[2048,224]{1,0:T(8,128)(2,1)} %bitcast.68, f32[2048,224]{0,1:T(8,128)} %fusion.28, bf16[3,224,2048]{2,1,0:T(8,128)(2,1)} %all-gather.5.cloned.1.call-done), kind=kOutput, calls=%fused_computation.12 | convolution fusion | flops 3760848896 | bytes 28966912 | tf_op jit(solution)/shard_map/dot_general | solution.py:48
  228.4 19.2 %add_convert_fusion = bf16[2048,2048]{1,0:T(8,128)(2,1)} fusion(f32[2048,2048]{1,0:T(8,128)} %fusion.6, f32[2048,2048]{1,0:T(8,128)} %fusion.7, f32[2048]{0:T(1024)S(1)} %bitcast.75, f32[2048]{0:T(1024)S(1)} %bitcast.76, f32[2048]{0:T(1024)S(1)} %bitcast.74, bf16[3,224,2048]{2,1,0:T(8,128)(2,1)} %all-gather.5.cloned.1.call-done, ...), kind=kOutput, calls=%fused_computation.4 | convolution fusion | flops 3786014720 | bytes 54157312 | tf_op jit(solution)/shard_map/dot_general | solution.py:48
  247.6 8.3 %copy.64 = bf16[4,4,2,64,2048]{4,3,2,1,0:T(8,128)(2,1)} copy(bf16[4,4,2,64,2048]{4,3,1,0,2:T(8,128)(2,1)} %bitcast.59) | data formatting | bytes 16777216 | tf_op jit(solution)/shard_map/transpose | solution.py:13
  255.8 0.0 reduce-scatter.4.cloned.1.call-update
  255.9 0.0 reduce-scatter.6.cloned.1.call-start
  255.9 81.5 %reduce-scatter.4.cloned.1.call-done = bf16[8,64,2048]{2,1,0:T(8,128)(2,1)} async-done(((bf16[32,64,2048]{2,1,0:T(8,128)(2,1)}), bf16[8,64,2048]{2,1,0:T(8,128)(2,1)}) %reduce-scatter.4.cloned.1.call-update) | async-done | bytes 2097168 | tf_op jit(solution)/shard_map/reduce_scatter | solution.py:16
  337.4 0.0 reduce-scatter.6.cloned.1.call-update
  337.5 0.0 reduce-scatter.8.cloned.1.call-start
  337.5 31.6 %reduce-scatter.6.cloned.1.call-done = bf16[2,64,2048]{2,1,0:T(8,128)(2,1)} async-done(((bf16[8,64,2048]{2,1,0:T(8,128)(2,1)}), bf16[2,64,2048]{2,1,0:T(8,128)(2,1)}) %reduce-scatter.6.cloned.1.call-update) | async-done | bytes 524304 | tf_op jit(solution)/shard_map/reduce_scatter | solution.py:16
  369.1 0.0 reduce-scatter.8.cloned.1.call-update
  369.1 11.4 %copy.69 = bf16[3,64,32,224]{3,1,2,0:T(8,128)(2,1)} copy(bf16[3,64,32,224]{1,0,3,2:T(4,128)(2,1)} %bitcast.57) | data formatting | bytes 5505024 | tf_op jit(solution)/shard_map/all_to_all | solution.py:72
  380.5 4.6 %copy.65 = bf16[3,2048,224]{1,2,0:T(8,128)(2,1)} copy(bf16[3,2048,224]{2,1,0:T(8,128)(2,1)} %bitcast.66) | data formatting | bytes 5505024
  385.1 2.7 copy.66
  387.7 1.1 reduce-scatter.8.cloned.1.call-done
  388.8 3.7 copy.72
  (5 shorter events, 0.1 us)
Async XLA Ops:
  7.2 100.2 %all-gather.3.cloned.1.call-start = ((), (), s32[]{:S(2)}) async-start(), calls=%async_computation.6 | async-start | bytes 3440640 | tf_op jit(solution)/shard_map/all_gather | solution.py:68
  11.9 54.6 %all-to-all-start = ((bf16[4,3,64,1792]{3,2,1,0:T(8,128)(2,1)}), bf16[4,3,64,1792]{3,2,1,0:T(8,128)(2,1)S(1)}, u32[]{:S(2)}, u32[]{:S(2)}) async-start(bf16[4,3,64,1792]{3,2,1,0:T(8,128)(2,1)} %stack.2), calls=%async_computation | async-start | bytes 5505024 | tf_op jit(solution)/shard_map/all_to_all | solution.py:63
  18.5 2.4 copy-start
  18.5 179.4 %all-gather.5.cloned.1.call-start = ((), (), s32[]{:S(2)}) async-start(), calls=%async_computation.7 | async-start | bytes 3440640 | tf_op jit(solution)/shard_map/all_gather | solution.py:69
  86.5 7.7 %copy-start.1 = (s32[1,2048,2]{1,2,0:T(2,128)S(1)}, s32[1,2048,2]{1,2,0:T(2,128)}, u32[]{:S(2)}) copy-start(s32[1,2048,2]{1,2,0:T(2,128)} %param.12) | copy-start | bytes 49156
  86.5 43.5 %all-to-all-start.1 = ((bf16[32,2,21504]{2,1,0:T(2,128)(2,1)}), bf16[32,2,21504]{2,1,0:T(2,128)(2,1)S(1)}, u32[]{:S(2)}, u32[]{:S(2)}) async-start(bf16[32,2,21504]{2,1,0:T(2,128)(2,1)} %reshape.115), calls=%async_computation.1 | async-start | bytes 5505024 | tf_op jit(solution)/shard_map/all_to_all | solution.py:72
  130.0 42.7 %all-to-all-start.2 = ((bf16[32,2,21504]{2,1,0:T(2,128)(2,1)}), bf16[32,2,21504]{2,1,0:T(2,128)(2,1)}, u32[]{:S(2)}, u32[]{:S(2)}) async-start(bf16[32,2,21504]{2,1,0:T(2,128)(2,1)} %reshape.117), calls=%async_computation.2 | async-start | bytes 5505024 | tf_op jit(solution)/shard_map/all_to_all | solution.py:73
  137.9 199.5 %reduce-scatter.4.cloned.1.call-start = ((), (), s32[]{:S(2)}) async-start(), calls=%async_computation.8 | async-start | bytes 10485760 | tf_op jit(solution)/shard_map/reduce_scatter | solution.py:16
  156.4 8.3 %slice-start = ((s8[8388608]{0:T(1024)(128)(4,1)}), s8[4194304]{0:T(1024)(128)(4,1)S(1)}, s32[]{:S(2)}) async-start(s8[8388608]{0:T(1024)(128)(4,1)} %bitcast.54), calls=%async_computation.11 | async-start | bytes 8388608
  157.0 7.7 %slice-start.1 = ((s8[8388608]{0:T(1024)(128)(4,1)}), s8[4194304]{0:T(1024)(128)(4,1)S(1)}, s32[]{:S(2)}) async-start(s8[8388608]{0:T(1024)(128)(4,1)} %bitcast.54), calls=%async_computation.12 | async-start | bytes 8388608
  255.9 113.2 %reduce-scatter.6.cloned.1.call-start = ((), (), s32[]{:S(2)}) async-start(), calls=%async_computation.9 | async-start | bytes 2621440 | tf_op jit(solution)/shard_map/reduce_scatter | solution.py:16
  337.5 51.3 %reduce-scatter.8.cloned.1.call-start = ((), (), s32[]{:S(2)}) async-start(), calls=%async_computation.10 | async-start | bytes 786432 | tf_op jit(solution)/shard_map/reduce_scatter | solution.py:16
Sparse Core Ops, SparseCore 0:
  10.2 48.8 all-gather.2
  60.8 29.6 all-gather.4
  256.0 81.4 reduce-scatter.3
  339.7 29.3 reduce-scatter.5
  371.9 16.8 reduce-scatter.7
